TPU v7x, 32 devices: a whole 2x2x4 slice. The times are simulated.
32 devices in a mesh: fs: 16 (over z, y, x), tp: 2 (over core).
Axes of the slice: x: 2, y: 2, z: 4, core: 2. Of those that a mesh axis runs over, the one named last changes fastest.
Arguments:
- sequence_entries: bfloat16 [4096, 2048], P('fs', 'tp'), may hold values from -6 to 6
- former_norm_factor: float32 [2048], replicated, may hold values from 0.1 to 1.9
- conveyor_matrix: float32 [2048, 1536], P('fs', 'tp'), may hold values from -0.125 to 0.125
- conveyor_rescalers: float32 [1536], P('tp'), may hold values from 0.3 to 3
- blend_value_matrix: float32 [2048, 1536], P('fs', 'tp'), may hold values from -0.125 to 0.125
- blend_rescalers: float32 [1536], P('tp'), may hold values from 0.18 to 4.8, as said below
- blend_norm_factor: float32 [1536], P('tp'), may hold values from 0.1 to 1.9
- location_matrices: bfloat16 [24, 128, 128], P('tp'), may hold values from -0.5 to 0.5
- location_offsets: float32 [24, 128], P('tp'), may hold values from 0.1 to 1.9
- branch_emission_matrix: float32 [1536, 2048], P('tp', 'fs'), may hold values from -0.15625 to 0.15625
- emission_rescalers: float32 [2048], P('fs'), may hold values from 0.3 to 3
- latter_norm_factor: float32 [2048], replicated, may hold values from 0.1 to 1.9
- valve_matrix: float32 [2048, 5632], P('fs', 'tp'), may hold values from -0.125 to 0.125
- valve_rescalers: float32 [5632], P('tp'), may hold values from 0.3 to 3
- raising_matrix: float32 [2048, 5632], P('fs', 'tp'), may hold values from -0.125 to 0.125
- raising_rescalers: float32 [5632], P('tp'), may hold values from 0.3 to 3
- lowering_matrix: float32 [5632, 2048], P('tp', 'fs'), may hold values from -0.078125 to 0.078125
- lowering_rescalers: float32 [2048], P('fs'), may hold values from 0.3 to 3
Outputs:
- layer_out: bfloat16 [4096, 2048], P('fs', 'tp')
Inputs may be any that keep to these rules, and one draw needn't show every extreme that they name: `blend_rescalers`: positive column scales.
All inputs are finite; a program needn't handle non-finite values.
Results may differ from a plain program's by a relative error of at most 0.02.
Values may be sent and summed in bfloat16 or wider, within the bound.
A program may use at most 128 MiB of HBM per device.

v0:
```python
import functools

import jax
import jax.numpy as jnp
from jax import lax
from jax.experimental import pallas as pl
from jax.experimental.pallas import tpu as pltpu
from jax.sharding import PartitionSpec as P

EPS = 1e-06
MESH = pl.DeviceIdType.MESH
BF = jnp.bfloat16
F32 = jnp.float32
SCHEDULE = {
    "a0": ("PWC",),
    "a2": ("YWCb", "ZWCa",),
    "a4": ("ZWCb", "PWE", "ZWEa", "PVB", "YWEa", "FWCa",),
    "a5": ("PVA", "ZWEb",),
    "b0": ("YWCa", "ZVBa",),
    "b1": ("FWCb",),
    "b3": ("YWEb",),
    "b4": ("FWEa",),
    "c0": ("ZVAa",),
    "c1": ("YVBa",),
    "c2": ("PLA", "FWEb",),
    "c3": ("YVAa", "FVBa",),
    "d0": ("ZLAa", "PLB", "YVAb",),
    "d1": ("ZVAb",),
    "d2": ("YLAa",),
    "d4": ("FVAa",),
    "d5": ("YLBa",),
    "e0": ("ZVBb", "YLBb",),
    "e1": ("YVBb", "ZLAb", "FVAb",),
    "e2": ("FVBb",),
    "f0": ("ZLBb",),
    "f1": ("ZLBa", "YLAb",),
    "f4": ("FLAb",),
    "g0": ("FLAa",),
    "f5": ("FLBb",),
    "g4": ("FLBa",),
}
SPLITS = (16, 12, 12, 9)


def layer_kernel(
    dims,
    x_in, g1_in, cv_in, sc_in, bv_in, sb_in, gb_in, loc_in, offs_in, em_in, es_in,
    g2_in, vv_in, sv_in, rv_in, sr_in, lw_in, ls_in,
    out,
    f_cv, f_bv, f_em, f_vv, f_rv, f_lw, loc,
    g1, g2, sc_all, sb_all, gb_all, sv_all, sr_all, es, ls, offs_all,
    s_wc, s_we, s_va, s_vb, s_la, s_lb,
    wc, we, va, vb, la, lb,
    xa, xm, nrm, car, sgn, gat, hid, sq, offs, part, half, rcore, rx, rz, dx_in, dz_in,
    inl, p1s, p1r, p1l, p2s, p2r, ags, agr, sqs, sqr, rss, rsr,
):
    rows, width, chan, ff, cut, block_len, group_width, total_chan, splits = dims
    fs = lax.axis_index("fs")
    c = lax.axis_index("tp")
    x = fs % 2
    y = (fs // 2) % 2
    zl = (fs // 4) % 2
    zh = fs // 8
    ai = x + 2 * zl
    groups = chan // group_width

    def dev(dx=0, dy=0, dzl=0, dzh=0, dc=0):
        nx = 1 - x if dx else x
        ny = 1 - y if dy else y
        nzl = 1 - zl if dzl else zl
        nzh = 1 - zh if dzh else zh
        nc = 1 - c if dc else c
        return {"fs": nzh * 8 + nzl * 4 + ny * 2 + nx, "tp": nc}

    def blk(da):
        return (1 - x if da & 1 else x) + 2 * (1 - zl if da & 2 else zl)

    loads = {}

    def load(name, src, dst):
        copy = pltpu.make_async_copy(src, dst, inl.at[len(loads)])
        copy.start()
        loads[name] = copy

    load("cv", cv_in, f_cv)
    load("bv", bv_in, f_bv)
    load("x", x_in, xa.at[c, ai])
    load("em", em_in, f_em)
    load("es", es_in, es.at[0])
    load("vv", vv_in, f_vv)
    load("rv", rv_in, f_rv)
    load("ls", ls_in, ls.at[0])
    load("lw", lw_in, f_lw)
    for name, src, dst in (
        ("g1", g1_in, g1.at[0]), ("sc", sc_in, sc_all.at[0]), ("sb", sb_in, sb_all.at[0]), ("gb", gb_in, gb_all.at[0]),
        ("offs", offs_in, offs_all), ("loc", loc_in.at[pl.ds(ai * groups, groups)], loc),
        ("g2", g2_in, g2.at[0]), ("sv", sv_in, sv_all.at[0]), ("sr", sr_in, sr_all.at[0]),
    ):
        load(name, src, dst)

    peers = [dev(dx=da & 1, dzl=da & 2, dc=dc) for da in range(4) for dc in range(2) if da or dc]
    peers += [dev(dy=1), dev(dzh=1)]
    barrier = pltpu.get_barrier_semaphore()
    for peer in peers:
        pl.semaphore_signal(barrier, inc=1, device_id=peer, device_id_type=MESH)

    loads["cv"].wait()
    loads["bv"].wait()
    for q in range(4):
        s_wc[q, :, :chan] = f_cv[:, q * chan:(q + 1) * chan].astype(BF)
        s_wc[q, :, chan:] = f_bv[:, q * chan:(q + 1) * chan].astype(BF)
    loads["x"].wait()
    pl.semaphore_wait(barrier, len(peers))

    def rcopy(src, dst, ss, rs, to):
        return pltpu.make_async_remote_copy(
            src_ref=src, dst_ref=dst, send_sem=ss, recv_sem=rs, device_id=to, device_id_type=MESH
        )

    pending = []

    def go(copy):
        copy.start()
        pending.append(copy)
        return copy

    ins = (s_wc, s_we, s_va, s_vb, s_la, s_lb)
    dst = (wc, we, va, vb, la, lb)
    rowwise = (False, True, False, False, True, True)
    WC, WE, VA, VB, LA, LB = range(6)

    def cell(m):
        if rowwise[m]:
            lanes = ins[m].shape[2]
            return dst[m].at[zh, zl, :, pl.ds(pl.multiple_of((y * 2 + x) * lanes, lanes), lanes)]
        return dst[m].at[zh, zl, y, x]

    def piece(m, a, b, h):
        level = 1 - zl if h == "b" else zl
        if rowwise[m]:
            lanes = 2 * ins[m].shape[2]
            return dst[m].at[a, level, :, pl.ds(pl.multiple_of(b * lanes, lanes), lanes)]
        return dst[m].at[a, level, b]

    first = {}
    second = {}

    def phase1(m):
        local = pltpu.make_async_copy(ins[m].at[ai], cell(m), p1l.at[m])
        local.start()
        copies = {
            da: go(rcopy(ins[m].at[blk(da)], cell(m), p1s.at[m, da - 1], p1r.at[m, da - 1], dev(dx=da & 1, dzl=da & 2)))
            for da in (3, 2, 1)
        }
        first[m, "a"] = (local, copies[1])
        first[m, "b"] = (copies[2], copies[3])

    def settle(m, h):
        if (m, h) in first:
            one, two = first.pop((m, h))
            two.wait_recv()
            if h == "a":
                one.wait()
            else:
                one.wait_recv()

    def send(kind, m, h):
        i = "ZYF".index(kind) * 2 + "ab".index(h)
        if kind == "F":
            second["Z", m, h].wait_recv()
            src = piece(m, 1 - zh, y, h)
        else:
            settle(m, h)
            src = piece(m, zh, y, h)
        to = dev(dzh=1) if kind == "Z" else dev(dy=1)
        second[kind, m, h] = go(rcopy(src, src, p2s.at[m, i], p2r.at[m, i], to))

    def ready(m, kinds="YF"):
        for kind in kinds:
            for h in "ab":
                second[kind, m, h].wait_recv()

    def gather_start(buf, k):
        own = buf.at[c, ai]
        z = go(rcopy(own, own, ags.at[k, 0], agr.at[k, 0], dev(dzl=1)))
        xx = go(rcopy(own, own, ags.at[k, 1], agr.at[k, 1], dev(dx=1)))
        core = go(rcopy(own, own, ags.at[k, 2], agr.at[k, 2], dev(dc=1)))
        return [z, xx, core]

    def norm_block(buf, gain, b):
        total = jnp.zeros((rows, 1), F32)
        for h in range(2):
            v = buf[h, b].astype(F32)
            total = total + jnp.sum(v * v, axis=-1, keepdims=True)
        factor = lax.rsqrt(total / (2 * width) + EPS)
        for h in range(2):
            nrm[h, b] = (buf[h, b].astype(F32) * factor * gain[:, h * width:(h + 1) * width]).astype(BF)

    def project(w, b):
        n = w.shape[-1]
        return jnp.dot(nrm[0, b], w[0].reshape(width, n), preferred_element_type=F32) + jnp.dot(
            nrm[1, b], w[1].reshape(width, n), preferred_element_type=F32
        )

    def emit(b):
        v = gat[b]
        n = we.shape[-1]
        for h in range(2):
            for q in range(2):
                part[h, b, :, q * n:(q + 1) * n] = jnp.dot(v, we[h, q], preferred_element_type=F32).astype(BF)

    def emit_plane(b, a, p):
        n = 2 * s_la.shape[2]
        lanes = pl.ds(pl.multiple_of(p * n, n), n)
        for q in range(2):
            at = pl.ds(pl.multiple_of(q * 2 * n + p * n, n), n)
            part[a, b, :, at] = (
                jnp.dot(hid[b, :, :cut], la[a, q, :, lanes], preferred_element_type=F32)
                + jnp.dot(hid[b, :, cut:], lb[a, q, :, lanes], preferred_element_type=F32)
            ).astype(BF)

    order = (3, 1, 2, 0)

    def scatter_cores(k):
        cores = {
            da: rcopy(part.at[1 - c, blk(da)], rcore.at[k, blk(da)], rss.at[k, i], rsr.at[k, i], dev(dc=1))
            for i, da in enumerate(order)
        }
        return cores

    def scatter_links(k):
        cutoff = splits[2 + k]
        rest = rows - cutoff
        top, bottom = pl.ds(0, cutoff), pl.ds(cutoff, rest)
        zb, xb, db = blk(2), blk(1), blk(3)
        links = {
            "dx": rcopy(half.at[k, db, top], dx_in.at[k, top], rss.at[k, 4], rsr.at[k, 4], dev(dx=1)),
            "x0": rcopy(half.at[k, xb, top], rx.at[k, top], rss.at[k, 7], rsr.at[k, 7], dev(dx=1)),
            "z1": rcopy(half.at[k, zb, top], rz.at[k, top], rss.at[k, 8], rsr.at[k, 8], dev(dzl=1)),
        }
        if rest:
            links["dz"] = rcopy(
                half.at[k, db, bottom], dz_in.at[k, bottom], rss.at[k, 5], rsr.at[k, 5], dev(dzl=1)
            )
            links["z0"] = rcopy(half.at[k, zb, bottom], rz.at[k, bottom], rss.at[k, 6], rsr.at[k, 6], dev(dzl=1))
            links["x1"] = rcopy(half.at[k, xb, bottom], rx.at[k, bottom], rss.at[k, 9], rsr.at[k, 9], dev(dx=1))
        pending.extend(links.values())
        return links, top, bottom

    def scatter_first(k, cores, plan):
        links, top, bottom = plan

        def combine(da):
            b = blk(da)
            cores[da].wait_recv()
            half[k, b] = (part[c, b].astype(F32) + rcore[k, b].astype(F32)).astype(BF)

        combine(3)
        links["dx"].start()
        if "dz" in links:
            links["dz"].start()
        combine(1)
        links["x0"].start()
        combine(2)
        if "z0" in links:
            links["z0"].start()

    def scatter_second(k, cores, plan, tag):
        links, top, bottom = plan
        zb, xb = blk(2), blk(1)
        slot_of(tag + "0")
        links["dx"].wait_recv()
        half[k, zb, top] = (half[k, zb, top].astype(F32) + dx_in[k, top].astype(F32)).astype(BF)
        links["z1"].start()
        if "dz" in links:
            links["dz"].wait_recv()
            half[k, xb, bottom] = (half[k, xb, bottom].astype(F32) + dz_in[k, bottom].astype(F32)).astype(BF)
            links["x1"].start()
        slot_of(tag + "1")
        cores[0].wait_recv()
        for da in order:
            cores[da].wait_send()
        own = part[c, ai].astype(F32) + rcore[k, ai].astype(F32)
        for name in ("x0", "z0", "z1", "x1"):
            if name in links:
                links[name].wait_recv()
        return own + rz[k].astype(F32) + rx[k].astype(F32)

    def pick(ref, n, lo, hi):
        value = ref[:, lo:hi]
        for k in range(1, 4):
            value = jnp.where(ai == k, ref[:, k * n + lo:k * n + hi], value)
        return value

    names = {"WC": WC, "WE": WE, "VA": VA, "VB": VB, "LA": LA, "LB": LB}

    def slot_of(name):
        for step in SCHEDULE.get(name, ()):
            m = names[step[1:3]]
            if step[0] == "P":
                phase1(m)
            else:
                send(step[0], m, step[3])

    def gather(buf, k, gain, st, tag, early, late):
        z, xx, core = st
        cutoff = splits[k]
        z.wait_recv()
        zb = buf.at[c, blk(2)]
        zbt = buf.at[c, blk(2), pl.ds(0, cutoff)]
        diag = [go(rcopy(zbt, zbt, ags.at[k, 3], agr.at[k, 3], dev(dx=1)))]
        zcore = go(rcopy(zb, zb, ags.at[k, 4], agr.at[k, 4], dev(dc=1)))
        slot_of(tag + "0")
        xx.wait_recv()
        xb = buf.at[c, blk(1)]
        if cutoff < rows:
            xbb = buf.at[c, blk(1), pl.ds(cutoff, rows - cutoff)]
            diag.append(go(rcopy(xbb, xbb, ags.at[k, 5], agr.at[k, 5], dev(dzl=1))))
        xcore = go(rcopy(xb, xb, ags.at[k, 6], agr.at[k, 6], dev(dc=1)))
        slot_of(tag + "1")
        core.wait_recv()
        norm_block(buf, gain, blk(0))
        slot_of(tag + "2")
        zcore.wait_recv()
        norm_block(buf, gain, blk(2))
        slot_of(tag + "3")
        xcore.wait_recv()
        norm_block(buf, gain, blk(1))
        slot_of(tag + "4")
        early()
        for copy in diag:
            copy.wait_recv()
        db = buf.at[c, blk(3)]
        dcore = go(rcopy(db, db, ags.at[k, 7], agr.at[k, 7], dev(dc=1)))
        slot_of(tag + "5")
        dcore.wait_recv()
        norm_block(buf, gain, blk(3))
        slot_of(tag + "6")
        late()

    slot_of("a0")
    st1 = gather_start(xa, 0)
    slot_of("a1")
    loads["em"].wait()
    loads["es"].wait()
    for q in range(4):
        s_we[q] = (f_em[q * chan:(q + 1) * chan] * es[...]).astype(BF)
    slot_of("a2")
    loads["vv"].wait()
    loads["rv"].wait()
    for q in range(4):
        base = q * ff
        s_va[q, :, :cut] = f_vv[:, base:base + cut].astype(BF)
        s_va[q, :, cut:] = f_rv[:, base:base + cut].astype(BF)
    slot_of("a3")
    for q in range(4):
        base = q * ff
        s_vb[q, :, :ff - cut] = f_vv[:, base + cut:base + ff].astype(BF)
        s_vb[q, :, ff - cut:] = f_rv[:, base + cut:base + ff].astype(BF)
    slot_of("a4")
    loads["ls"].wait()
    loads["lw"].wait()
    for q in range(4):
        base = q * ff
        s_la[q] = (f_lw[base:base + cut] * ls[...]).astype(BF)
        s_lb[q] = (f_lw[base + cut:base + ff] * ls[...]).astype(BF)
    slot_of("a5")
    for name in ("g1", "sc", "sb", "gb", "offs", "loc", "g2", "sv", "sr"):
        loads[name].wait()
    head = lax.broadcasted_iota(jnp.int32, (offs_all.shape[0], chan), 0)
    lane = lax.broadcasted_iota(jnp.int32, (offs_all.shape[0], chan), 1)
    chosen = (lane >= (head - ai * groups) * group_width) & (lane < (head - ai * groups + 1) * group_width)
    offs[...] = lax.dot_general(
        offs_all[...], chosen.astype(F32), (((0,), (0,)), ((), ())),
        precision=lax.Precision.HIGHEST, preferred_element_type=F32,
    )
    slot = ai * 2 + c

    def first_projection(da):
        b = blk(da)
        sc, sb, gb = (pick(v, chan, 0, chan) for v in (sc_all, sb_all, gb_all))
        both = project(wc, b)
        car[b] = jax.nn.gelu(both[:, :chan] * sc)
        signal = jax.nn.gelu(both[:, chan:] * sb)
        sgn[b] = (signal * gb).astype(BF)
        sq[slot, b] = lax.dot_general(
            jnp.ones((8, chan), F32), signal * signal, (((1,), (1,)), ((), ())),
            precision=lax.Precision.HIGHEST, preferred_element_type=F32,
        )

    def first_early():
        ready(WC)
        slot_of("c0")
        for i, da in enumerate((0, 2, 1)):
            first_projection(da)
            slot_of(f"c{i + 1}")

    def first_late():
        first_projection(3)
        slot_of("c4")

    gather(xa, 0, g1, st1, "b", first_early, first_late)
    squares = []
    for da in range(4):
        for dc in range(2):
            if da or dc:
                i = da * 2 + dc - 1
                squares.append(
                    go(rcopy(sq.at[slot], sq.at[slot], sqs.at[i], sqr.at[i], dev(dx=da & 1, dzl=da & 2, dc=dc)))
                )
    slot_of("d0")
    for copy in squares:
        copy.wait_recv()
    slot_of("d1")
    lower = lax.broadcasted_iota(jnp.int32, (block_len, block_len), 0) >= lax.broadcasted_iota(
        jnp.int32, (block_len, block_len), 1
    )
    lane = lax.broadcasted_iota(jnp.int32, (block_len, chan), 1)
    cores1 = scatter_cores(0)
    ready(WE)
    for i, da in enumerate(order):
        b = blk(da)
        total = sq[0, b]
        for j in range(1, 8):
            total = total + sq[j, b]
        factor = lax.rsqrt(total / total_chan + EPS)
        for s in range(rows // block_len):
            span = slice(s * block_len, (s + 1) * block_len)
            values = sgn[b, span]
            mixed = jnp.zeros((block_len, chan), F32)
            for g in range(groups):
                mat = jnp.where(lower, loc[g].astype(F32), 0.0) * factor[0:1, span]
                one = jnp.dot(mat.astype(BF), values, preferred_element_type=F32)
                inside = (lane >= g * group_width) & (lane < (g + 1) * group_width)
                mixed = jnp.where(inside, one, mixed)
            gat[b, span] = (car[b, span] * (mixed + offs[...])).astype(BF)
        emit(b)
        cores1[da].start()
        slot_of(f"d{i + 2}")
    plan1 = scatter_links(0)
    scatter_first(0, cores1, plan1)
    summed = scatter_second(0, cores1, plan1, "e")
    xm[c, ai] = (xa[c, ai].astype(F32) + summed).astype(BF)
    st2 = gather_start(xm, 1)
    slot_of("e2")

    def up_projection(w, lo, hi, da):
        b = blk(da)
        sv, sr = (pick(v, ff, lo, hi) for v in (sv_all, sr_all))
        both = project(w, b)
        gate = both[:, :hi - lo] * sv
        up = both[:, hi - lo:] * sr
        hid[b, :, lo:hi] = (jax.nn.silu(gate) * up).astype(BF)

    ups = ((VA, va, 0, cut, "g"), (VB, vb, cut, ff, "h"))

    def second_early():
        for m, w, lo, hi, tag in ups:
            ready(m)
            slot_of(tag + "0")
            for i, da in enumerate((0, 2, 1)):
                up_projection(w, lo, hi, da)
                slot_of(f"{tag}{i + 1}")

    def second_late():
        for m, w, lo, hi, tag in ups:
            up_projection(w, lo, hi, 3)
            slot_of(tag + "4")

    gather(xm, 1, g2, st2, "f", second_early, second_late)
    cores2 = scatter_cores(1)
    plan2 = scatter_links(1)
    for far in range(2):
        a = 1 - zh if far else zh
        for off in range(2):
            p = 1 - y if off else y
            if off:
                for m in (LA, LB):
                    ready(m, "YF"[far])
            for i, da in enumerate(order):
                emit_plane(blk(da), a, p)
                if off:

                    @pl.when(c != a)
                    def _():
                        cores2[da].start()

            if not far:
                slot_of(f"i{off}")

        @pl.when(c == a)
        def _():
            scatter_first(1, cores2, plan2)

    summed = scatter_second(1, cores2, plan2, "j")
    out[...] = (xm[c, ai].astype(F32) + summed).astype(BF)
    for copy in pending:
        copy.wait_send()


def on_device_fused(
    sequence_entries, former_norm_factor, conveyor_matrix, conveyor_rescalers,
    blend_value_matrix, blend_rescalers, blend_norm_factor, location_matrices,
    location_offsets, branch_emission_matrix, emission_rescalers, latter_norm_factor,
    valve_matrix, valve_rescalers, raising_matrix, raising_rescalers,
    lowering_matrix, lowering_rescalers,
):
    parts = 4
    rows, width = sequence_entries.shape
    depth, chans = conveyor_matrix.shape
    chan = chans // parts
    hidden = valve_matrix.shape[1]
    ff = hidden // parts
    cut = (ff // 2 + 127) // 128 * 128
    heads = location_matrices.shape[0]
    groups = heads // parts
    block_len = location_matrices.shape[1]
    group_width = chan // groups
    total_chan = chans * lax.axis_size("tp")
    cols = branch_emission_matrix.shape[1]
    args = (
        sequence_entries, former_norm_factor, conveyor_matrix, conveyor_rescalers,
        blend_value_matrix, blend_rescalers, blend_norm_factor, location_matrices,
        location_offsets, branch_emission_matrix, emission_rescalers, latter_norm_factor,
        valve_matrix, valve_rescalers, raising_matrix, raising_rescalers,
        lowering_matrix, lowering_rescalers,
    )
    vm = pltpu.VMEM
    dma = pltpu.SemaphoreType.DMA
    cube = (2, 2, 2, 2, depth)
    scratch = [
        vm((depth, chans), F32), vm((depth, chans), F32), vm((chans, cols), F32),
        vm((depth, hidden), F32), vm((depth, hidden), F32), vm((hidden, cols), F32),
        vm((groups, block_len, block_len), BF),
        vm((1, 2 * width), F32), vm((1, 2 * width), F32), vm((1, chans), F32), vm((1, chans), F32),
        vm((1, chans), F32), vm((1, hidden), F32), vm((1, hidden), F32), vm((1, cols), F32),
        vm((1, cols), F32), vm((heads, block_len), F32),
        vm((parts, depth, 2 * chan), BF), vm((parts, chan, cols), BF),
        vm((parts, depth, 2 * cut), BF), vm((parts, depth, 2 * (ff - cut)), BF),
        vm((parts, cut, cols), BF), vm((parts, ff - cut, cols), BF),
        vm(cube + (2 * chan,), BF), vm((2, 2, chan, 4 * cols), BF),
        vm(cube + (2 * cut,), BF), vm(cube + (2 * (ff - cut),), BF),
        vm((2, 2, cut, 4 * cols), BF), vm((2, 2, ff - cut, 4 * cols), BF),
        vm((2, 4, rows, width), BF), vm((2, 4, rows, width), BF), vm((2, 4, rows, width), BF),
        vm((4, rows, chan), F32), vm((4, rows, chan), BF), vm((4, rows, chan), BF),
        vm((4, rows, ff), BF), vm((8, 4, 8, rows), F32), vm((block_len, chan), F32),
        vm((2, 4, rows, width), BF), vm((2, 4, rows, width), BF), vm((2, 4, rows, width), BF),
        vm((2, rows, width), BF), vm((2, rows, width), BF),
        vm((2, rows, width), BF), vm((2, rows, width), BF),
        dma((18,)), dma((6, 3)), dma((6, 3)), dma((6,)), dma((6, 6)), dma((6, 6)),
        dma((2, 8)), dma((2, 8)), dma((7,)), dma((7,)), dma((2, 10)), dma((2, 10)),
    ]
    splits = tuple(rows * part // 16 for part in SPLITS)
    dims = (rows, width, chan, ff, cut, block_len, group_width, total_chan, splits)
    return pl.pallas_call(
        functools.partial(layer_kernel, dims),
        out_shape=jax.ShapeDtypeStruct((rows, width), BF),
        in_specs=[pl.BlockSpec(memory_space=pl.ANY)] * len(args),
        out_specs=pl.BlockSpec(memory_space=pltpu.VMEM),
        scratch_shapes=scratch,
        compiler_params=pltpu.CompilerParams(
            collective_id=0, has_side_effects=True, vmem_limit_bytes=66000000
        ),
    )(*args)


def normalize(rows, gain):
    values = rows.astype(jnp.float32)
    factor = lax.rsqrt(jnp.mean(values * values, axis=-1, keepdims=True) + EPS)
    return (values * factor * gain).astype(jnp.bfloat16)


def elementwise_plus(left_rows, pieces):
    return (
        jnp.dot(left_rows, pieces[0], preferred_element_type=jnp.float32),
        jnp.dot(left_rows, pieces[1], preferred_element_type=jnp.float32),
    )


def project_cols(left_rows, scales, piece):
    return jnp.dot(left_rows, piece, preferred_element_type=jnp.float32) * scales


def on_device(
    sequence_entries,
    former_norm_factor,
    conveyor_matrix,
    conveyor_rescalers,
    blend_value_matrix,
    blend_rescalers,
    blend_norm_factor,
    location_matrices,
    location_offsets,
    branch_emission_matrix,
    emission_rescalers,
    latter_norm_factor,
    valve_matrix,
    valve_rescalers,
    raising_matrix,
    raising_rescalers,
    lowering_matrix,
    lowering_rescalers,
):
    out_scales, down_scales = (
        lax.all_gather(emission_rescalers, "fs", axis=0, tiled=True),
        lax.all_gather(lowering_rescalers, "fs", axis=0, tiled=True),
    )
    full_rows = lax.all_gather(sequence_entries, "tp", axis=1, tiled=True)
    own_width = sequence_entries.shape[1]
    own_start = lax.axis_index("tp") * own_width
    standardized_source = normalize(full_rows, former_norm_factor)
    conveyor_prior, stream_prior = elementwise_plus(
        standardized_source,
        (
            lax.all_gather(conveyor_matrix.astype(jnp.bfloat16), "fs", axis=0, tiled=True),
            lax.all_gather(blend_value_matrix.astype(jnp.bfloat16), "fs", axis=0, tiled=True),
        ),
    )
    conveyor_current = jax.nn.gelu(conveyor_prior * conveyor_rescalers)
    signal = jax.nn.gelu(stream_prior * blend_rescalers)
    total_sq = lax.psum(jnp.sum(signal * signal, axis=1), "tp")
    channels = signal.shape[1] * lax.axis_size("tp")
    signal_norm = (
        signal * lax.rsqrt(total_sq / channels + EPS)[:, None] * blend_norm_factor
    ).astype(jnp.bfloat16)
    local_groups = location_matrices.shape[0]
    block_len = location_matrices.shape[1]
    group_width = signal.shape[1] // local_groups
    lower_mask = jnp.tril(jnp.ones((block_len, block_len), bool))
    masked = jnp.where(lower_mask[None], location_matrices, jnp.zeros((), jnp.bfloat16))
    signal_blocks = signal_norm.reshape(-1, block_len, local_groups, group_width)
    location_blended = jnp.einsum(
        "gts,bsgd->btgd", masked, signal_blocks, preferred_element_type=jnp.float32
    )
    location_blended = location_blended + location_offsets.T[None, :, :, None]
    filtered_result = (conveyor_current * location_blended.reshape(conveyor_current.shape)).astype(
        jnp.bfloat16
    )
    mixer_terms = project_cols(
        filtered_result,
        out_scales,
        lax.all_gather(branch_emission_matrix.astype(jnp.bfloat16), "fs", axis=1, tiled=True),
    )
    summed = lax.psum(mixer_terms.astype(jnp.bfloat16), "tp").astype(jnp.float32)
    mid_rows = (full_rows.astype(jnp.float32) + summed).astype(jnp.bfloat16)
    mid_own = lax.dynamic_slice_in_dim(mid_rows, own_start, own_width, 1)
    ffn_in = normalize(mid_rows, latter_norm_factor)
    gate_half = valve_matrix.astype(jnp.bfloat16)
    up_half = raising_matrix.astype(jnp.bfloat16)
    whole_gate, whole_up = (
        lax.all_gather(gate_half, "fs", axis=0, tiled=True),
        lax.all_gather(up_half, "fs", axis=0, tiled=True),
    )
    pre_gate = jnp.dot(ffn_in, whole_gate, preferred_element_type=jnp.float32)
    pre_up = jnp.dot(ffn_in, whole_up, preferred_element_type=jnp.float32)
    hidden = (jax.nn.silu(pre_gate * valve_rescalers) * (pre_up * raising_rescalers)).astype(
        jnp.bfloat16
    )
    ffn_terms = project_cols(
        hidden,
        down_scales,
        lax.all_gather(lowering_matrix.astype(jnp.bfloat16), "fs", axis=1, tiled=True),
    )
    ffn_share = lax.psum_scatter(
        ffn_terms.astype(jnp.bfloat16), "tp", scatter_dimension=1, tiled=True
    ).astype(jnp.float32)
    return (mid_own.astype(jnp.float32) + ffn_share).astype(jnp.bfloat16)


def solution(mesh):
    sizes = dict(mesh.shape)
    fused = sizes["tp"] == 2 and sizes["fs"] == 16
    return jax.shard_map(
        on_device_fused if fused else on_device,
        mesh=mesh,
        in_specs=(
            P("fs", "tp"),
            P(),
            P("fs", "tp"),
            P("tp"),
            P("fs", "tp"),
            P("tp"),
            P("tp"),
            P("tp", None, None),
            P("tp", None),
            P("tp", "fs"),
            P("fs"),
            P(),
            P("fs", "tp"),
            P("tp"),
            P("fs", "tp"),
            P("tp"),
            P("tp", "fs"),
            P("fs"),
        ),
        out_specs=P("fs", "tp"),
        check_vma=False,
    )
```

profile of v0, /device:TPU:1, one launch (start us, length us, event | category | flops | bytes accessed | tf_op | source)
XLA Modules:
  0.0 177.3 jit_solution(13352952931044366119)
XLA Ops:
  0.0 175.4 %shard_map.172 = bf16[256,1024]{1,0:T(8,128)(2,1)} custom-call(bf16[256,1024]{1,0:T(8,128)(2,1)} %x_in.1, f32[2048]{0:T(1024)} %g1_in.1, f32[128,768]{1,0:T(8,128)} %cv_in.1, f32[768]{0:T(1024)} %sc_in.1, f32[128,768]{1,0:T(8,128)} %bv_in.1, f32[768]{0:T(1024)} %sb_in.1, f32[768]{0:T(1024)} %gb_in.1, bf16[12,128,128]{2,1,0:T(8,128)(2,1)} %loc_in.1, ...), custom_call_target="tpu_custom_call" | custom-call | tf_op jit(solution)/shard_map/pallas_call | solution.py:555
  175.4 1.9 %copy.20 = bf16[256,1024]{1,0:T(8,128)(2,1)} copy(bf16[256,1024]{1,0:T(8,128)(2,1)} %shard_map.172) | data formatting | bytes 1048576
where the time goes:
time: 177 us
  Pallas kernels  175 us (99%)
  local copies, waits for them, and re-layouts  1.87 us (1%)
    pallas_call x1, Pallas kernels, on_device_fused(): pl.pallas_call(functools.partial(layer_kernel, dims), out_shape=jax.Shape...  175 us

commit v1 on v0

--- a/solution.py
+++ b/solution.py
@@ -13,33 +13,29 @@
 F32 = jnp.float32
 SCHEDULE = {
     "a0": ("PWC",),
-    "a2": ("YWCb", "ZWCa",),
-    "a4": ("ZWCb", "PWE", "ZWEa", "PVB", "YWEa", "FWCa",),
-    "a5": ("PVA", "ZWEb",),
-    "b0": ("YWCa", "ZVBa",),
-    "b1": ("FWCb",),
-    "b3": ("YWEb",),
-    "b4": ("FWEa",),
-    "c0": ("ZVAa",),
-    "c1": ("YVBa",),
-    "c2": ("PLA", "FWEb",),
-    "c3": ("YVAa", "FVBa",),
-    "d0": ("ZLAa", "PLB", "YVAb",),
-    "d1": ("ZVAb",),
-    "d2": ("YLAa",),
-    "d4": ("FVAa",),
-    "d5": ("YLBa",),
-    "e0": ("ZVBb", "YLBb",),
-    "e1": ("YVBb", "ZLAb", "FVAb",),
-    "e2": ("FVBb",),
+    "a4": ("PVA", "LWC", "HWC", "XWC",),
+    "a5": ("PVB", "YVAa", "UWC",),
+    "b0": ("PWE", "ZVAb",),
+    "b1": ("MWC", "VWC", "ZVAa",),
+    "b2": ("XWE", "YVBa", "HWE",),
+    "b3": ("YVAb", "PLA", "LWE",),
+    "b4": ("QWC", "FVAb",),
+    "b5": ("FVAa",),
+    "c0": ("ZLAb", "VWE",),
+    "c1": ("YLAa", "MWE", "ZVBa",),
+    "c2": ("UWE",),
+    "d0": ("ZVBb", "YVBb", "PLB",),
+    "d1": ("YLBa", "QWE",),
+    "e1": ("FVBa",),
+    "e2": ("ZLBa", "FLAb", "YLAb", "FVBb",),
     "f0": ("ZLBb",),
-    "f1": ("ZLBa", "YLAb",),
-    "f4": ("FLAb",),
-    "g0": ("FLAa",),
-    "f5": ("FLBb",),
-    "g4": ("FLBa",),
+    "g0": ("FLBa",),
+    "g2": ("ZLAa",),
+    "g3": ("YLBb",),
+    "f6": ("FLBb",),
+    "i1": ("FLAa",),
 }
-SPLITS = (16, 12, 12, 9)
+SPLITS = (9, 9)
 
 
 def layer_kernel(
@@ -51,8 +47,8 @@
     g1, g2, sc_all, sb_all, gb_all, sv_all, sr_all, es, ls, offs_all,
     s_wc, s_we, s_va, s_vb, s_la, s_lb,
     wc, we, va, vb, la, lb,
-    xa, xm, nrm, car, sgn, gat, hid, sq, offs, part, half, rcore, rx, rz, dx_in, dz_in,
-    inl, p1s, p1r, p1l, p2s, p2r, ags, agr, sqs, sqr, rss, rsr,
+    xa, xm, nrm, car, sgn, gat, hid, sq, offs, part, half, rcore, rx, rz, dx_in, dz_in, mhalf, mcore, ry,
+    inl, p1s, p1r, p1l, p2s, p2r, ags, agr, sqs, sqr, rss, rsr, ws, wr, xs, xr, ms, mr,
 ):
     rows, width, chan, ff, cut, block_len, group_width, total_chan, splits = dims
     fs = lax.axis_index("fs")
@@ -84,7 +80,7 @@
 
     load("cv", cv_in, f_cv)
     load("bv", bv_in, f_bv)
-    load("x", x_in, xa.at[c, ai])
+    load("x", x_in, xa.at[c, y])
     load("em", em_in, f_em)
     load("es", es_in, es.at[0])
     load("vv", vv_in, f_vv)
@@ -93,20 +89,20 @@
     load("lw", lw_in, f_lw)
     for name, src, dst in (
         ("g1", g1_in, g1.at[0]), ("sc", sc_in, sc_all.at[0]), ("sb", sb_in, sb_all.at[0]), ("gb", gb_in, gb_all.at[0]),
-        ("offs", offs_in, offs_all), ("loc", loc_in.at[pl.ds(ai * groups, groups)], loc),
+        ("offs", offs_in, offs_all), ("loc", loc_in.at[pl.ds(y * groups, groups)], loc),
         ("g2", g2_in, g2.at[0]), ("sv", sv_in, sv_all.at[0]), ("sr", sr_in, sr_all.at[0]),
     ):
         load(name, src, dst)
 
     peers = [dev(dx=da & 1, dzl=da & 2, dc=dc) for da in range(4) for dc in range(2) if da or dc]
-    peers += [dev(dy=1), dev(dzh=1)]
+    peers += [dev(dy=1), dev(dy=1, dc=1), dev(dzh=1)]
     barrier = pltpu.get_barrier_semaphore()
     for peer in peers:
         pl.semaphore_signal(barrier, inc=1, device_id=peer, device_id_type=MESH)
 
     loads["cv"].wait()
     loads["bv"].wait()
-    for q in range(4):
+    for q in range(2):
         s_wc[q, :, :chan] = f_cv[:, q * chan:(q + 1) * chan].astype(BF)
         s_wc[q, :, chan:] = f_bv[:, q * chan:(q + 1) * chan].astype(BF)
     loads["x"].wait()
@@ -130,10 +126,46 @@
     WC, WE, VA, VB, LA, LB = range(6)
 
     def cell(m):
+        if m == WE:
+            lanes = ins[m].shape[2]
+            return we.at[zh, zl, x, :, pl.ds(pl.multiple_of(y * lanes, lanes), lanes)]
         if rowwise[m]:
             lanes = ins[m].shape[2]
             return dst[m].at[zh, zl, :, pl.ds(pl.multiple_of((y * 2 + x) * lanes, lanes), lanes)]
         return dst[m].at[zh, zl, y, x]
+
+    def level(m, a, b):
+        return we.at[a, b, x] if m == WE else wc.at[a, b, :, x]
+
+    first = {}
+    moved = {}
+    landed = set()
+
+    def mixer_send(kind, m):
+        i = "PLHXMUVQ".index(kind)
+
+        def move(src, to, into=None):
+            moved[kind, m] = go(rcopy(src, src if into is None else into, ws.at[m, i], wr.at[m, i], to))
+
+        if kind == "P":
+            first[m] = pltpu.make_async_copy(ins[m].at[y], cell(m), p1l.at[m])
+            first[m].start()
+            move(ins[m].at[1 - y], dev(dy=1), cell(m))
+            return
+        if m in first:
+            first.pop(m).wait()
+            moved["P", m].wait_recv()
+        source = {"U": "L", "V": "H", "M": "H", "Q": "M"}.get(kind)
+        if source and (source, m) not in landed:
+            landed.add((source, m))
+            moved[source, m].wait_recv()
+        far, other = kind in "MVQ", kind in "UQ"
+        src = level(m, 1 - zh if far else zh, 1 - zl if other else zl)
+        move(src, dev(dzh=1) if kind == "H" else dev(dzl=1) if kind in "LM" else dev(dx=1))
+
+    def mixer_ready(m):
+        for kind in "XUVQ":
+            moved[kind, m].wait_recv()
 
     def piece(m, a, b, h):
         level = 1 - zl if h == "b" else zl
@@ -142,7 +174,6 @@
             return dst[m].at[a, level, :, pl.ds(pl.multiple_of(b * lanes, lanes), lanes)]
         return dst[m].at[a, level, b]
 
-    first = {}
     second = {}
 
     def phase1(m):
@@ -204,10 +235,14 @@
 
     def emit(b):
         v = gat[b]
-        n = we.shape[-1]
+        n = s_we.shape[-1]
         for h in range(2):
             for q in range(2):
-                part[h, b, :, q * n:(q + 1) * n] = jnp.dot(v, we[h, q], preferred_element_type=F32).astype(BF)
+                for xx in range(2):
+                    both = jnp.dot(v, we[h, q, xx], preferred_element_type=F32).astype(BF)
+                    for yy in range(2):
+                        at = ((q * 2 + yy) * 2 + xx) * n
+                        part[h, b, :, at:at + n] = both[:, yy * n:(yy + 1) * n]
 
     def emit_plane(b, a, p):
         n = 2 * s_la.shape[2]
@@ -229,7 +264,7 @@
         return cores
 
     def scatter_links(k):
-        cutoff = splits[2 + k]
+        cutoff = splits[1 + k]
         rest = rows - cutoff
         top, bottom = pl.ds(0, cutoff), pl.ds(cutoff, rest)
         zb, xb, db = blk(2), blk(1), blk(3)
@@ -288,8 +323,8 @@
 
     def pick(ref, n, lo, hi):
         value = ref[:, lo:hi]
-        for k in range(1, 4):
-            value = jnp.where(ai == k, ref[:, k * n + lo:k * n + hi], value)
+        for k in range(1, ref.shape[1] // n):
+            value = jnp.where((ai if ref.shape[1] // n == 4 else y) == k, ref[:, k * n + lo:k * n + hi], value)
         return value
 
     names = {"WC": WC, "WE": WE, "VA": VA, "VB": VB, "LA": LA, "LB": LB}
@@ -297,7 +332,9 @@
     def slot_of(name):
         for step in SCHEDULE.get(name, ()):
             m = names[step[1:3]]
-            if step[0] == "P":
+            if m in (WC, WE):
+                mixer_send(step[0], m)
+            elif step[0] == "P":
                 phase1(m)
             else:
                 send(step[0], m, step[3])
@@ -339,11 +376,13 @@
         late()
 
     slot_of("a0")
-    st1 = gather_start(xa, 0)
+    own = xa.at[c, y]
+    xnear = go(rcopy(own, own, xs.at[0], xr.at[0], dev(dy=1)))
+    xcore = go(rcopy(own, own, xs.at[1], xr.at[1], dev(dc=1)))
     slot_of("a1")
     loads["em"].wait()
     loads["es"].wait()
-    for q in range(4):
+    for q in range(2):
         s_we[q] = (f_em[q * chan:(q + 1) * chan] * es[...]).astype(BF)
     slot_of("a2")
     loads["vv"].wait()
@@ -369,16 +408,27 @@
         loads[name].wait()
     head = lax.broadcasted_iota(jnp.int32, (offs_all.shape[0], chan), 0)
     lane = lax.broadcasted_iota(jnp.int32, (offs_all.shape[0], chan), 1)
-    chosen = (lane >= (head - ai * groups) * group_width) & (lane < (head - ai * groups + 1) * group_width)
+    chosen = (lane >= (head - y * groups) * group_width) & (lane < (head - y * groups + 1) * group_width)
     offs[...] = lax.dot_general(
         offs_all[...], chosen.astype(F32), (((0,), (0,)), ((), ())),
         precision=lax.Precision.HIGHEST, preferred_element_type=F32,
     )
-    slot = ai * 2 + c
-
-    def first_projection(da):
-        b = blk(da)
-        sc, sb, gb = (pick(v, chan, 0, chan) for v in (sc_all, sb_all, gb_all))
+    slot = y * 2 + c
+    xcore.wait_recv()
+    norm_block(xa, g1, y)
+    slot_of("b0")
+    xnear.wait_recv()
+    near = xa.at[c, 1 - y]
+    xlast = go(rcopy(near, near, xs.at[2], xr.at[2], dev(dc=1)))
+    slot_of("b1")
+    xlast.wait_recv()
+    norm_block(xa, g1, 1 - y)
+    for name in ("b2", "b3", "b4", "b5"):
+        slot_of(name)
+    mixer_ready(WC)
+    slot_of("c0")
+    sc, sb, gb = (pick(v, chan, 0, chan) for v in (sc_all, sb_all, gb_all))
+    for i, b in enumerate((y, 1 - y)):
         both = project(wc, b)
         car[b] = jax.nn.gelu(both[:, :chan] * sc)
         signal = jax.nn.gelu(both[:, chan:] * sb)
@@ -387,27 +437,11 @@
             jnp.ones((8, chan), F32), signal * signal, (((1,), (1,)), ((), ())),
             precision=lax.Precision.HIGHEST, preferred_element_type=F32,
         )
-
-    def first_early():
-        ready(WC)
-        slot_of("c0")
-        for i, da in enumerate((0, 2, 1)):
-            first_projection(da)
-            slot_of(f"c{i + 1}")
-
-    def first_late():
-        first_projection(3)
-        slot_of("c4")
-
-    gather(xa, 0, g1, st1, "b", first_early, first_late)
-    squares = []
-    for da in range(4):
-        for dc in range(2):
-            if da or dc:
-                i = da * 2 + dc - 1
-                squares.append(
-                    go(rcopy(sq.at[slot], sq.at[slot], sqs.at[i], sqr.at[i], dev(dx=da & 1, dzl=da & 2, dc=dc)))
-                )
+        slot_of(f"c{i + 1}")
+    squares = [
+        go(rcopy(sq.at[slot], sq.at[slot], sqs.at[i], sqr.at[i], dev(dy=dy, dc=dc)))
+        for i, (dy, dc) in enumerate(((1, 0), (1, 1), (0, 1)))
+    ]
     slot_of("d0")
     for copy in squares:
         copy.wait_recv()
@@ -415,33 +449,46 @@
     lower = lax.broadcasted_iota(jnp.int32, (block_len, block_len), 0) >= lax.broadcasted_iota(
         jnp.int32, (block_len, block_len), 1
     )
-    lane = lax.broadcasted_iota(jnp.int32, (block_len, chan), 1)
-    cores1 = scatter_cores(0)
-    ready(WE)
-    for i, da in enumerate(order):
-        b = blk(da)
+    pack = max(1, 128 // group_width)
+    wide = pack * group_width
+    lane = lax.broadcasted_iota(jnp.int32, (block_len, wide), 1)
+    mixer_ready(WE)
+    slot_of("d2")
+    cores1 = {}
+    for i, b in enumerate((1 - y, y)):
         total = sq[0, b]
-        for j in range(1, 8):
+        for j in range(1, 4):
             total = total + sq[j, b]
         factor = lax.rsqrt(total / total_chan + EPS)
         for s in range(rows // block_len):
             span = slice(s * block_len, (s + 1) * block_len)
-            values = sgn[b, span]
-            mixed = jnp.zeros((block_len, chan), F32)
-            for g in range(groups):
-                mat = jnp.where(lower, loc[g].astype(F32), 0.0) * factor[0:1, span]
-                one = jnp.dot(mat.astype(BF), values, preferred_element_type=F32)
-                inside = (lane >= g * group_width) & (lane < (g + 1) * group_width)
-                mixed = jnp.where(inside, one, mixed)
-            gat[b, span] = (car[b, span] * (mixed + offs[...])).astype(BF)
+            for j in range(groups // pack):
+                lanes = slice(j * wide, (j + 1) * wide)
+                values = sgn[b, span, lanes]
+                mixed = jnp.zeros((block_len, wide), F32)
+                for g in range(pack):
+                    mat = jnp.where(lower, loc[j * pack + g].astype(F32), 0.0) * factor[0:1, span]
+                    one = jnp.dot(mat.astype(BF), values, preferred_element_type=F32)
+                    inside = (lane >= g * group_width) & (lane < (g + 1) * group_width)
+                    mixed = jnp.where(inside, one, mixed)
+                gat[b, span, lanes] = (car[b, span, lanes] * (mixed + offs[:, lanes])).astype(BF)
         emit(b)
-        cores1[da].start()
-        slot_of(f"d{i + 2}")
-    plan1 = scatter_links(0)
-    scatter_first(0, cores1, plan1)
-    summed = scatter_second(0, cores1, plan1, "e")
-    xm[c, ai] = (xa[c, ai].astype(F32) + summed).astype(BF)
-    st2 = gather_start(xm, 1)
+        cores1[i] = rcopy(part.at[1 - c, b], mcore.at[b], ms.at[i], mr.at[i], dev(dc=1))
+        cores1[i].start()
+        if i == 0:
+            slot_of("d3")
+    cores1[0].wait_recv()
+    mhalf[...] = (part[c, 1 - y].astype(F32) + mcore[1 - y].astype(F32)).astype(BF)
+    across = go(rcopy(mhalf, ry, ms.at[2], mr.at[2], dev(dy=1)))
+    slot_of("e0")
+    cores1[1].wait_recv()
+    slot_of("e1")
+    across.wait_recv()
+    for i in range(2):
+        cores1[i].wait_send()
+    summed = part[c, y].astype(F32) + mcore[y].astype(F32) + ry[...].astype(F32)
+    xm[c, ai] = (xa[c, y].astype(F32) + summed).astype(BF)
+    st2 = gather_start(xm, 0)
     slot_of("e2")
 
     def up_projection(w, lo, hi, da):
@@ -467,9 +514,9 @@
             up_projection(w, lo, hi, 3)
             slot_of(tag + "4")
 
-    gather(xm, 1, g2, st2, "f", second_early, second_late)
-    cores2 = scatter_cores(1)
-    plan2 = scatter_links(1)
+    gather(xm, 0, g2, st2, "f", second_early, second_late)
+    cores2 = scatter_cores(0)
+    plan2 = scatter_links(0)
     for far in range(2):
         a = 1 - zh if far else zh
         for off in range(2):
@@ -490,9 +537,9 @@
 
         @pl.when(c == a)
         def _():
-            scatter_first(1, cores2, plan2)
-
-    summed = scatter_second(1, cores2, plan2, "j")
+            scatter_first(0, cores2, plan2)
+
+    summed = scatter_second(0, cores2, plan2, "j")
     out[...] = (xm[c, ai].astype(F32) + summed).astype(BF)
     for copy in pending:
         copy.wait_send()
@@ -508,12 +555,12 @@
     parts = 4
     rows, width = sequence_entries.shape
     depth, chans = conveyor_matrix.shape
-    chan = chans // parts
+    chan = chans // 2
     hidden = valve_matrix.shape[1]
     ff = hidden // parts
     cut = (ff // 2 + 127) // 128 * 128
     heads = location_matrices.shape[0]
-    groups = heads // parts
+    groups = heads // 2
     block_len = location_matrices.shape[1]
     group_width = chan // groups
     total_chan = chans * lax.axis_size("tp")
@@ -535,20 +582,22 @@
         vm((1, 2 * width), F32), vm((1, 2 * width), F32), vm((1, chans), F32), vm((1, chans), F32),
         vm((1, chans), F32), vm((1, hidden), F32), vm((1, hidden), F32), vm((1, cols), F32),
         vm((1, cols), F32), vm((heads, block_len), F32),
-        vm((parts, depth, 2 * chan), BF), vm((parts, chan, cols), BF),
+        vm((2, depth, 2 * chan), BF), vm((2, chan, cols), BF),
         vm((parts, depth, 2 * cut), BF), vm((parts, depth, 2 * (ff - cut)), BF),
         vm((parts, cut, cols), BF), vm((parts, ff - cut, cols), BF),
-        vm(cube + (2 * chan,), BF), vm((2, 2, chan, 4 * cols), BF),
+        vm(cube + (2 * chan,), BF), vm((2, 2, 2, chan, 2 * cols), BF),
         vm(cube + (2 * cut,), BF), vm(cube + (2 * (ff - cut),), BF),
         vm((2, 2, cut, 4 * cols), BF), vm((2, 2, ff - cut, 4 * cols), BF),
-        vm((2, 4, rows, width), BF), vm((2, 4, rows, width), BF), vm((2, 4, rows, width), BF),
-        vm((4, rows, chan), F32), vm((4, rows, chan), BF), vm((4, rows, chan), BF),
-        vm((4, rows, ff), BF), vm((8, 4, 8, rows), F32), vm((block_len, chan), F32),
-        vm((2, 4, rows, width), BF), vm((2, 4, rows, width), BF), vm((2, 4, rows, width), BF),
-        vm((2, rows, width), BF), vm((2, rows, width), BF),
-        vm((2, rows, width), BF), vm((2, rows, width), BF),
+        vm((2, 2, rows, width), BF), vm((2, 4, rows, width), BF), vm((2, 4, rows, width), BF),
+        vm((2, rows, chan), F32), vm((2, rows, chan), BF), vm((2, rows, chan), BF),
+        vm((4, rows, ff), BF), vm((4, 2, 8, rows), F32), vm((block_len, chan), F32),
+        vm((2, 4, rows, width), BF), vm((1, 4, rows, width), BF), vm((1, 4, rows, width), BF),
+        vm((1, rows, width), BF), vm((1, rows, width), BF),
+        vm((1, rows, width), BF), vm((1, rows, width), BF),
+        vm((rows, width), BF), vm((2, rows, width), BF), vm((rows, width), BF),
         dma((18,)), dma((6, 3)), dma((6, 3)), dma((6,)), dma((6, 6)), dma((6, 6)),
-        dma((2, 8)), dma((2, 8)), dma((7,)), dma((7,)), dma((2, 10)), dma((2, 10)),
+        dma((1, 8)), dma((1, 8)), dma((3,)), dma((3,)), dma((1, 10)), dma((1, 10)),
+        dma((2, 8)), dma((2, 8)), dma((3,)), dma((3,)), dma((3,)), dma((3,)),
     ]
     splits = tuple(rows * part // 16 for part in SPLITS)
     dims = (rows, width, chan, ff, cut, block_len, group_width, total_chan, splits)

time: 177 us -> 172 us (0.972)
  Pallas kernels: 175 us -> 170 us
    pallas_call x1, Pallas kernels: 175 us -> 170 us  [on_device_fused(): pl.pallas_call(functools.partial(layer_kernel, dims), out_shape=jax.Shape...]
where the time goes in v1:
time: 172 us
  Pallas kernels  170 us (99%)
  local copies, waits for them, and re-layouts  1.87 us (1%)
    pallas_call x1, Pallas kernels, on_device_fused(): pl.pallas_call(functools.partial(layer_kernel, dims), out_shape=jax.Shape...  170 us

profile of v1, /device:TPU:1, one launch (start us, length us, event | category | flops | bytes accessed | tf_op | source)
XLA Modules:
  0.0 171.7 jit_solution(11497184157825333278)
XLA Ops:
  0.0 169.8 %shard_map.172 = bf16[256,1024]{1,0:T(8,128)(2,1)} custom-call(bf16[256,1024]{1,0:T(8,128)(2,1)} %x_in.1, f32[2048]{0:T(1024)} %g1_in.1, f32[128,768]{1,0:T(8,128)} %cv_in.1, f32[768]{0:T(1024)} %sc_in.1, f32[128,768]{1,0:T(8,128)} %bv_in.1, f32[768]{0:T(1024)} %sb_in.1, f32[768]{0:T(1024)} %gb_in.1, bf16[12,128,128]{2,1,0:T(8,128)(2,1)} %loc_in.1, ...), custom_call_target="tpu_custom_call" | custom-call | tf_op jit(solution)/shard_map/pallas_call | solution.py:604
  169.8 1.9 %copy.20 = bf16[256,1024]{1,0:T(8,128)(2,1)} copy(bf16[256,1024]{1,0:T(8,128)(2,1)} %shard_map.172) | data formatting | bytes 1048576

commit v2 on v1

--- a/solution.py
+++ b/solution.py
@@ -13,29 +13,31 @@
 F32 = jnp.float32
 SCHEDULE = {
     "a0": ("PWC",),
-    "a4": ("PVA", "LWC", "HWC", "XWC",),
-    "a5": ("PVB", "YVAa", "UWC",),
-    "b0": ("PWE", "ZVAb",),
-    "b1": ("MWC", "VWC", "ZVAa",),
-    "b2": ("XWE", "YVBa", "HWE",),
-    "b3": ("YVAb", "PLA", "LWE",),
-    "b4": ("QWC", "FVAb",),
-    "b5": ("FVAa",),
-    "c0": ("ZLAb", "VWE",),
-    "c1": ("YLAa", "MWE", "ZVBa",),
-    "c2": ("UWE",),
-    "d0": ("ZVBb", "YVBb", "PLB",),
-    "d1": ("YLBa", "QWE",),
-    "e1": ("FVBa",),
-    "e2": ("ZLBa", "FLAb", "YLAb", "FVBb",),
-    "f0": ("ZLBb",),
-    "g0": ("FLBa",),
-    "g2": ("ZLAa",),
-    "g3": ("YLBb",),
-    "f6": ("FLBb",),
+    "a3": ("PVA", "XWC",),
+    "a4": ("HWC", "PWE", "LWC",),
+    "a5": ("MWC",),
+    "b0": ("VWC", "ZVAb",),
+    "b1": ("PVB", "YVAb", "UWC",),
+    "b2": ("YVAa", "QWC",),
+    "b3": ("HWE", "FVAb",),
+    "b4": ("ZVAa", "YVBa", "XWE",),
+    "b5": ("MWE", "YVBb",),
+    "c0": ("LWE",),
+    "c1": ("ZVBb", "PLB",),
+    "c2": ("VWE",),
+    "d0": ("ZVBa", "QWE", "FVAa", "UWE",),
+    "d2": ("YLBa",),
+    "d3": ("PLA",),
+    "e0": ("YLAb", "YLAa", "FVBa", "FVBb",),
+    "e1": ("ZLBb",),
+    "e2": ("ZLAb",),
+    "f1": ("YLBb", "FLBb",),
+    "f2": ("ZLBa", "ZLAa",),
+    "g1": ("FLAb",),
+    "f6": ("FLBa",),
     "i1": ("FLAa",),
 }
-SPLITS = (9, 9)
+SPLITS = (9, 8)
 
 
 def layer_kernel(

time: 172 us -> 168 us (0.977)
  Pallas kernels: 170 us -> 166 us
    pallas_call x1, Pallas kernels: 170 us -> 166 us  [on_device_fused(): pl.pallas_call(functools.partial(layer_kernel, dims), out_shape=jax.Shape...]
where the time goes in v2:
time: 168 us
  Pallas kernels  166 us (99%)
  local copies, waits for them, and re-layouts  1.87 us (1%)
    pallas_call x1, Pallas kernels, on_device_fused(): pl.pallas_call(functools.partial(layer_kernel, dims), out_shape=jax.Shape...  166 us

profile of v2, /device:TPU:1, one launch (start us, length us, event | category | flops | bytes accessed | tf_op | source)
XLA Modules:
  0.0 167.9 jit_solution(12891668339147423762)
XLA Ops:
  0.0 166.0 %shard_map.172 = bf16[256,1024]{1,0:T(8,128)(2,1)} custom-call(bf16[256,1024]{1,0:T(8,128)(2,1)} %x_in.1, f32[2048]{0:T(1024)} %g1_in.1, f32[128,768]{1,0:T(8,128)} %cv_in.1, f32[768]{0:T(1024)} %sc_in.1, f32[128,768]{1,0:T(8,128)} %bv_in.1, f32[768]{0:T(1024)} %sb_in.1, f32[768]{0:T(1024)} %gb_in.1, bf16[12,128,128]{2,1,0:T(8,128)(2,1)} %loc_in.1, ...), custom_call_target="tpu_custom_call" | custom-call | tf_op jit(solution)/shard_map/pallas_call | solution.py:606
  166.0 1.9 %copy.20 = bf16[256,1024]{1,0:T(8,128)(2,1)} copy(bf16[256,1024]{1,0:T(8,128)(2,1)} %shard_map.172) | data formatting | bytes 1048576
